TPU v7x, 32 devices: a whole 2x2x4 slice. The times are simulated.
32 devices in a mesh: ep: 16 (over z, y, x), tp: 2 (over core).
Axes of the slice: x: 2, y: 2, z: 4, core: 2. Of those that a mesh axis runs over, the one named last changes fastest.
Arguments:
- tokens: bfloat16 [256, 1024], P('ep'), may hold values from -6 to 6
- mixer_gain: float32 [1024], replicated, may hold values from 0.1 to 1.9
- query_weight: bfloat16 [1024, 1024], P(None, 'tp'), may hold values from -0.1875 to 0.1875
- key_weight: bfloat16 [1024, 256], P(None, 'tp'), may hold values from -0.1875 to 0.1875
- value_weight: bfloat16 [1024, 256], P(None, 'tp'), may hold values from -0.1875 to 0.1875
- head_lambda: float32 [8], P('tp'), may hold values from 0.3 to 0.8
- head_gain: float32 [128], replicated, may hold values from 0.1 to 1.9
- out_weight: bfloat16 [1024, 1024], P('tp'), may hold values from -0.1875 to 0.1875
- cache_keys: bfloat16 [256, 1024, 256], P('ep', None, 'tp'), may hold values from -700 to 700
- cache_values: bfloat16 [256, 1024, 256], P('ep', None, 'tp'), may hold values from -6 to 6
- seq_lengths: int32 [256], P('ep'), may hold values from 2 to 1024, as said below
- channel_gain: float32 [1024], replicated, may hold values from 0.1 to 1.9
- expert_ids: int32 [256, 6], P('ep'), may hold values from 0 to 15, all different within a row; in each aligned block of 16 rows (0 to 15, 16 to 31, ...) at most 12 rows name the same one
- expert_shares: bfloat16 [256, 6], P('ep'), may hold values from 0.19921875 to 1
- expert_gate: bfloat16 [16, 1024, 256], P('ep', None, 'tp'), may hold values from -0.1875 to 0.1875
- expert_up: bfloat16 [16, 1024, 256], P('ep', None, 'tp'), may hold values from -0.1875 to 0.1875
- expert_down: bfloat16 [16, 256, 1024], P('ep', 'tp'), may hold values from -0.375 to 0.375
- dense_gate: bfloat16 [1024, 4096], P('tp', 'ep'), may hold values from -0.1875 to 0.1875
- dense_up: bfloat16 [1024, 4096], P('tp', 'ep'), may hold values from -0.1875 to 0.1875
- dense_down: bfloat16 [4096, 1024], P('ep', 'tp'), may hold values from -0.1875 to 0.1875
- branch_gate: float32 [1024], replicated, may hold values from -0.1875 to 0.1875
Outputs:
- layer_out: bfloat16 [256, 1024], P('ep', 'tp')
Inputs may be any that keep to these rules, and one draw needn't show every extreme that they name: `expert_ids`: each row names 6 different experts; among the 16 rows of one index of ep no expert is named by more than 12 rows. `seq_lengths`: some sequence has all 1024 positions live.
All inputs are finite; a program needn't handle non-finite values.
Results may differ from a plain program's by a relative error of at most 0.017.
The roundings to bfloat16 on the way count: a program that leaves them out, or rounds other values in their place, can miss the bound.
Values may be sent and summed in bfloat16 or wider, within the bound.
A program may use at most 64 MiB of HBM per device.

v0:
```python
import jax
import jax.numpy as jnp
from jax import lax
from jax.sharding import PartitionSpec as P

HD = 64
NORM_EPS = 1e-06
HEAD_EPS = 1e-05
THETA = 500000.0
LAMBDA_BASE = 0.2


def norm_rows(values, gain_vec, epsilon):
    mean_square = jnp.mean(values * values, axis=-1, keepdims=True)
    return values * lax.rsqrt(mean_square + epsilon) * gain_vec


def rotate(values, position):
    half_dim = HD // 2
    frequency = THETA ** (-jnp.arange(half_dim, dtype=jnp.float32) * (2.0 / HD))
    angles = position.astype(jnp.float32)[:, None] * frequency[None, :]
    cos_vals = jnp.cos(angles)[:, None, :]
    sin_vals = jnp.sin(angles)[:, None, :]
    first_half = values[..., :half_dim]
    second = values[..., half_dim:]
    return jnp.concatenate(
        [first_half * cos_vals - second * sin_vals, second * cos_vals + first_half * sin_vals],
        axis=-1,
    )


def expert_rows(arrived, expert_gate, expert_up, expert_down):
    source_count, slot_count, model_width = arrived.shape
    stacked = arrived.reshape(source_count * slot_count, model_width)
    gate_part = jnp.dot(stacked, expert_gate[0], preferred_element_type=jnp.float32)
    up_part = jnp.dot(stacked, expert_up[0], preferred_element_type=jnp.float32)
    expert_hidden = (jax.nn.silu(gate_part) * up_part).astype(jnp.bfloat16)
    partial_value = jnp.dot(expert_hidden, expert_down[0], preferred_element_type=jnp.float32)
    partial_value = partial_value.reshape(source_count, slot_count, model_width)
    return lax.psum_scatter(
        partial_value.astype(jnp.bfloat16), "tp", scatter_dimension=2, tiled=True
    )


def dense_branch(partials, dense_down):
    summed = lax.psum(partials.astype(jnp.bfloat16), "tp").astype(jnp.float32)
    unit_count = partials.shape[1] // 2
    dense_hidden = (jax.nn.silu(summed[:, :unit_count]) * summed[:, unit_count:]).astype(
        jnp.bfloat16
    )
    return jnp.dot(dense_hidden, dense_down, preferred_element_type=jnp.float32)


def shards(
    tokens,
    mixer_gain,
    query_weight,
    key_weight,
    value_weight,
    head_lambda,
    head_gain,
    out_weight,
    cache_keys,
    cache_values,
    seq_lengths,
    channel_gain,
    expert_ids,
    expert_shares,
    expert_gate,
    expert_up,
    expert_down,
    dense_gate,
    dense_up,
    dense_down,
    branch_gate,
):
    seq_count, model_width = tokens.shape
    resid = tokens.astype(jnp.float32)
    normed = norm_rows(resid, mixer_gain, NORM_EPS).astype(jnp.bfloat16)
    value_width = 2 * HD
    groups = cache_values.shape[2] // value_width
    local_heads = head_lambda.shape[0]
    per_group = local_heads // groups
    cache_span = cache_keys.shape[1]
    query_raw = jnp.dot(normed, query_weight, preferred_element_type=jnp.float32).reshape(
        seq_count, local_heads * 2, HD
    )
    key_raw = jnp.dot(normed, key_weight, preferred_element_type=jnp.float32).reshape(
        seq_count, groups * 2, HD
    )
    value_new = jnp.dot(normed, value_weight, preferred_element_type=jnp.float32).astype(
        jnp.bfloat16
    )
    value_new = value_new.reshape(seq_count, groups, value_width)
    query = (
        rotate(query_raw, seq_lengths)
        .astype(jnp.bfloat16)
        .reshape(seq_count, groups, per_group, 2, HD)
    )
    key_new = rotate(key_raw, seq_lengths).astype(jnp.bfloat16).reshape(seq_count, groups, 2, HD)
    key_rows = cache_keys.reshape(seq_count, cache_span, groups, 2, HD)
    value_rows = cache_values.reshape(seq_count, cache_span, groups, value_width)
    lambdas = head_lambda.reshape(groups, per_group)
    score_scale = HD ** (-0.5)
    scores = (
        jnp.einsum("sgjcd,slgcd->sgjcl", query, key_rows, preferred_element_type=jnp.float32)
        * score_scale
    )
    fresh_score = (
        jnp.einsum("sgjcd,sgcd->sgjc", query, key_new, preferred_element_type=jnp.float32)
        * score_scale
    )
    live = jnp.arange(cache_span)[None, :] < seq_lengths[:, None]
    scores = jnp.where(live[:, None, None, None, :], scores, -jnp.inf)
    peak = jnp.maximum(jnp.max(scores, axis=-1), fresh_score)
    expo_scores = jnp.exp(scores - peak[..., None])
    expo_fresh = jnp.exp(fresh_score - peak)
    denom_sum = jnp.sum(expo_scores, axis=-1) + expo_fresh
    probability = expo_scores / denom_sum[..., None]
    prob_fresh = expo_fresh / denom_sum
    weight = (probability[:, :, :, 0] - lambdas[None, :, :, None] * probability[:, :, :, 1]).astype(
        jnp.bfloat16
    )
    weight_fresh = (prob_fresh[..., 0] - lambdas[None] * prob_fresh[..., 1]).astype(jnp.bfloat16)
    head_mix = jnp.einsum("sgjl,slgv->sgjv", weight, value_rows, preferred_element_type=jnp.float32)
    head_mix = (
        head_mix
        + weight_fresh.astype(jnp.float32)[..., None] * value_new.astype(jnp.float32)[:, :, None, :]
    )
    head_mix = head_mix.reshape(seq_count, local_heads, value_width)
    head_out = (norm_rows(head_mix, head_gain, HEAD_EPS) * (1.0 - LAMBDA_BASE)).astype(jnp.bfloat16)
    attn_part = jnp.dot(
        head_out.reshape(seq_count, local_heads * value_width),
        out_weight,
        preferred_element_type=jnp.float32,
    )
    attn_sum = lax.psum(attn_part.astype(jnp.bfloat16), "tp").astype(jnp.float32)
    resid_mid = (resid + attn_sum).astype(jnp.bfloat16)
    ffn_input = norm_rows(resid_mid.astype(jnp.float32), channel_gain, NORM_EPS).astype(
        jnp.bfloat16
    )
    gate_own = jax.nn.sigmoid(
        jnp.dot(ffn_input.astype(jnp.float32), branch_gate, precision=lax.Precision.HIGHEST)
    )
    half_width = model_width // lax.axis_size("tp")
    offset = lax.axis_index("tp") * half_width
    mid_half = lax.dynamic_slice_in_dim(resid_mid, offset, half_width, 1)
    experts_total = lax.axis_size("ep")
    top_count = expert_ids.shape[1]
    capacity = max(2, 2 * seq_count * top_count // experts_total)
    slot_ids = jnp.arange(1, capacity + 1, dtype=jnp.int32)
    named_mask = expert_ids[:, :, None] == jnp.arange(experts_total, dtype=jnp.int32)[None, None, :]
    picked = jnp.any(named_mask, axis=1)
    share_wide = expert_shares.astype(jnp.float32)[:, :, None]
    row_share = jnp.sum(jnp.where(named_mask, share_wide, jnp.zeros_like(share_wide)), axis=1)
    slot_rank = jnp.cumsum(picked.astype(jnp.int32), axis=0)
    placed = picked[None, :, :] & (slot_rank[None, :, :] == slot_ids[:, None, None])
    outgoing = jnp.einsum(
        "cse,sd->ecd", placed.astype(jnp.bfloat16), ffn_input, preferred_element_type=jnp.float32
    ).astype(jnp.bfloat16)
    expert_out = expert_rows(
        lax.all_to_all(outgoing, "ep", split_axis=0, concat_axis=0, tiled=True),
        expert_gate,
        expert_up,
        expert_down,
    )
    returned = lax.all_to_all(expert_out, "ep", split_axis=0, concat_axis=0, tiled=True)
    routed_sum = jnp.einsum(
        "cse,ecd->sd",
        placed.astype(jnp.float32) * row_share[None],
        returned.astype(jnp.float32),
        precision=lax.Precision.HIGHEST,
    )
    input_half = lax.dynamic_slice_in_dim(ffn_input, offset, half_width, 1)
    piece_rows = lax.all_gather(input_half, "ep", axis=0, tiled=True)
    partials = jnp.concatenate(
        [
            jnp.dot(piece_rows, dense_gate, preferred_element_type=jnp.float32),
            jnp.dot(piece_rows, dense_up, preferred_element_type=jnp.float32),
        ],
        axis=1,
    )
    branch_term = dense_branch(partials, dense_down)
    summed = lax.psum_scatter(branch_term, "ep", scatter_dimension=0, tiled=True)
    summed = gate_own[:, None] * summed + routed_sum
    return (mid_half.astype(jnp.float32) + summed).astype(jnp.bfloat16)


def solution(mesh):
    placed = (
        P("ep", None),
        P(),
        P(None, "tp"),
        P(None, "tp"),
        P(None, "tp"),
        P("tp"),
        P(),
        P("tp", None),
        P("ep", None, "tp"),
        P("ep", None, "tp"),
        P("ep"),
        P(),
        P("ep", None),
        P("ep", None),
        P("ep", None, "tp"),
        P("ep", None, "tp"),
        P("ep", "tp", None),
        P("tp", "ep"),
        P("tp", "ep"),
        P("ep", "tp"),
        P(),
    )
    return jax.shard_map(
        shards, mesh=mesh, in_specs=placed, out_specs=P("ep", "tp"), check_vma=False
    )
```

profile of v0, /device:TPU:0, one launch (start us, length us, event | category | flops | bytes accessed | tf_op | source)
XLA Modules:
  0.0 203.1 jit_solution(3398508565920873563)
XLA Ops:
  6.5 0.7 convert_element_type.100
  7.3 0.7 iota_compare_fusion
  8.0 0.9 fusion.32
  8.9 1.2 fusion.59
  10.2 1.6 fusion.61
  12.3 0.2 fusion.45
  12.6 6.4 %copy.65 = bf16[16,1024,128]{1,2,0:T(8,128)(2,1)} copy(bf16[16,1024,128]{2,1,0:T(8,128)(2,1)} %param.29) | data formatting | bytes 8388608 | tf_op args[8]
  19.1 3.0 %fusion.65 = (f32[16,4,2]{1,2,0:T(2,128)S(1)}, f32[16,1,4,2,1024]{4,2,3,0,1:T(4,128)S(1)}) fusion(bf16[16,1024,2,64]{1,3,2,0:T(8,128)(2,1)} %bitcast.151, bf16[16,4,2,32]{3,1,2,0:T(4,128)(2,1)S(1)} %copy.64, bf16[16,4,2,32]{3,1,2,0:T(4,128)(2,1)S(1)} %copy.63, pred[16,1024]{1,0:T(8,128)(4,1)S(1)} %iota_compare_fusion), kind=kOutput, calls=%fused_computation.106 | convolution fusion | flops 17203072 | bytes 4751872 | tf_op jit(solution)/shard_map/sgjcd,slgcd->sgjcl/dot_general | solution.py:106
  22.3 0.3 fusion.13
  22.9 0.3 fusion.12
  23.4 0.2 fusion.7
  23.6 3.0 %multiply_reduce_fusion = (f32[16,4]{1,0:T(8,128)S(1)}, f32[16,4,128]{2,1,0:T(4,128)S(1)}) fusion(f32[16,128]{1,0:T(8,128)S(1)} %fusion.7, f32[16,4]{1,0:T(8,128)S(1)} %copy.71, bf16[16,1024,128]{2,1,0:T(8,128)(2,1)} %param.30, f32[16,1,4,2,1024]{4,2,3,0,1:T(4,128)S(1)} %fusion.12, f32[4]{0:T(128)S(1)} %copy-done.9), kind=kOutput, calls=%fused_computation.69 | convolution fusion | flops 17006528 | bytes 4760080 | tf_op jit(solution)/shard_map/sgjl,slgv->sgjv/dot_general | solution.py:125
  26.7 0.2 convolution_convert_fusion.3
  27.0 3.7 %psum.14 = bf16[16,1024]{1,0:T(8,128)(2,1)S(1)} all-reduce(bf16[16,1024]{1,0:T(8,128)(2,1)S(1)} %convolution_convert_fusion.3), channel_id=1, replica_groups=mesh['ep'=16,'tp'=2] {'tp'}, use_global_device_ids=true, to_apply=%region_4.5 | all-reduce | flops 16384 | bytes 65536 | tf_op jit(solution)/shard_map/psum | solution.py:137
  31.3 0.2 fusion.66
  31.6 1.0 copy.73
  32.6 8.2 %all-to-all-start = ((bf16[16,12,1024]{2,1,0:T(8,128)(2,1)}), bf16[16,12,1024]{2,1,0:T(8,128)(2,1)S(1)}, u32[]{:S(2)}, u32[]{:S(2)}) async-start(bf16[16,12,1024]{2,1,0:T(8,128)(2,1)} %copy.73), calls=%async_computation.1 | async-start | bytes 1048576 | tf_op jit(solution)/shard_map/all_to_all | solution.py:162
  40.9 44.5 %all_gather.3 = bf16[256,512]{1,0:T(8,128)(2,1)S(1)} all-gather(bf16[16,512]{1,0:T(8,128)(2,1)S(1)} %constant_dynamic-slice_fusion), channel_id=1, replica_groups=mesh['ep'=16,'tp'=2] {'ep'}, dimensions={0}, use_global_device_ids=true | all-gather | bytes 278528 | tf_op jit(solution)/shard_map/all_gather | solution.py:175
  85.3 0.3 convolution_convert_fusion.1
  85.6 0.3 convolution_convert_fusion.2
  85.9 0.7 pad_maximum_fusion
  86.8 0.2 fusion.20
  87.1 0.3 fusion.3
  87.4 1.0 convolution_convert_fusion
  88.5 13.9 %all-reduce.2.cloned.1.call-done = bf16[256,512]{0,1:T(8,128)(2,1)} async-done(((bf16[256,512]{0,1:T(8,128)(2,1)}), bf16[256,512]{0,1:T(8,128)(2,1)}) %all-reduce.2.cloned.1.call-update) | async-done | bytes 262160 | tf_op jit(solution)/shard_map/psum | solution.py:46
  102.3 1.0 convert_element_type.112
  103.3 1.1 fusion.24
  104.4 9.2 %reduce-scatter.5.cloned.1.call-done = bf16[16,12,512]{2,0,1:T(8,128)(2,1)} async-done(((bf16[16,12,1024]{2,0,1:T(8,128)(2,1)}), bf16[16,12,512]{2,0,1:T(8,128)(2,1)}) %reduce-scatter.5.cloned.1.call-update) | async-done | bytes 196624 | tf_op jit(solution)/shard_map/reduce_scatter | solution.py:40
  113.7 1.7 copy.75
  115.4 6.7 %all-to-all-start.1 = ((bf16[16,12,512]{2,1,0:T(8,128)(2,1)}), bf16[16,12,512]{2,1,0:T(8,128)(2,1)S(1)}, u32[]{:S(2)}, u32[]{:S(2)}) async-start(bf16[16,12,512]{2,1,0:T(8,128)(2,1)} %copy.75), calls=%async_computation.3 | async-start | bytes 524288 | tf_op jit(solution)/shard_map/all_to_all | solution.py:167
  122.4 72.4 %reduce-scatter.3.cloned.1.call-done = f32[16,512]{1,0:T(8,128)} async-done(((f32[256,512]{1,0:T(8,128)}), f32[16,512]{1,0:T(8,128)}) %reduce-scatter.3.cloned.1.call-update) | async-done | bytes 32784 | tf_op jit(solution)/shard_map/reduce_scatter | solution.py:184
  194.8 1.8 fusion.6
  (79 shorter events, 2.5 us)
Async XLA Ops:
  6.5 20.2 %copy-start = (bf16[512,1024]{1,0:T(8,128)(2,1)S(1)}, bf16[512,1024]{1,0:T(8,128)(2,1)}, u32[]{:S(2)}) copy-start(bf16[512,1024]{1,0:T(8,128)(2,1)} %param.28) | copy-start | bytes 3145732
  19.1 4.1 %copy-start.9 = (f32[4]{0:T(128)S(1)}, f32[4]{0:T(128)}, u32[]{:S(2)}) copy-start(f32[4]{0:T(128)} %param.26) | copy-start | bytes 52
  19.1 4.3 %copy-start.1 = (bf16[16,1024]{1,0:T(8,128)(2,1)S(1)}, bf16[16,1024]{1,0:T(8,128)(2,1)}, u32[]{:S(2)}) copy-start(bf16[16,1024]{1,0:T(8,128)(2,1)} %param.21) | copy-start | bytes 98308
  19.1 4.3 %copy-start.7 = (f32[1024]{0:T(1024)S(1)}, f32[1024]{0:T(1024)}, u32[]{:S(2)}) copy-start(f32[1024]{0:T(1024)} %param.22) | copy-start | bytes 12292
  19.1 4.3 %copy-start.12 = (bf16[1024,128]{1,0:T(8,128)(2,1)S(1)}, bf16[1024,128]{1,0:T(8,128)(2,1)}, u32[]{:S(2)}) copy-start(bf16[1024,128]{1,0:T(8,128)(2,1)} %param.25) | copy-start | bytes 786436
  22.1 4.5 %copy-start.11 = (f32[128]{0:T(128)S(1)}, f32[128]{0:T(128)}, u32[]{:S(2)}) copy-start(f32[128]{0:T(128)} %param.27) | copy-start | bytes 1540
  22.1 8.8 %copy-start.6 = (s32[16,6]{0,1:T(8,128)S(1)}, s32[16,6]{0,1:T(8,128)}, u32[]{:S(2)}) copy-start(s32[16,6]{0,1:T(8,128)} %param.33) | copy-start | bytes 1156
  22.1 9.1 %copy-start.8 = (f32[1024]{0:T(1024)S(1)}, f32[1024]{0:T(1024)}, u32[]{:S(2)}) copy-start(f32[1024]{0:T(1024)} %param.32) | copy-start | bytes 12292
  23.6 61.8 %copy-start.3 = (bf16[512,256]{1,0:T(8,128)(2,1)S(1)}, bf16[512,256]{1,0:T(8,128)(2,1)}, u32[]{:S(2)}) copy-start(bf16[512,256]{1,0:T(8,128)(2,1)} %param.39) | copy-start | bytes 786436
  26.6 59.0 %copy-start.4 = (bf16[512,256]{1,0:T(8,128)(2,1)S(1)}, bf16[512,256]{1,0:T(8,128)(2,1)}, u32[]{:S(2)}) copy-start(bf16[512,256]{1,0:T(8,128)(2,1)} %param.38) | copy-start | bytes 786436
  26.7 60.1 %copy-start.2 = (bf16[1,1024,128]{2,1,0:T(8,128)(2,1)S(1)}, bf16[1,1024,128]{2,1,0:T(8,128)(2,1)}, u32[]{:S(2)}) copy-start(bf16[1,1024,128]{2,1,0:T(8,128)(2,1)} %param.35) | copy-start | bytes 786436
  30.7 56.4 %copy-start.13 = (bf16[1,1024,128]{2,1,0:T(8,128)(2,1)S(1)}, bf16[1,1024,128]{2,1,0:T(8,128)(2,1)}, u32[]{:S(2)}) copy-start(bf16[1,1024,128]{2,1,0:T(8,128)(2,1)} %param.36) | copy-start | bytes 786436
  31.6 55.8 %copy-start.5 = (bf16[1,128,1024]{2,1,0:T(8,128)(2,1)S(1)}, bf16[1,128,1024]{2,1,0:T(8,128)(2,1)}, u32[]{:S(2)}) copy-start(bf16[1,128,1024]{2,1,0:T(8,128)(2,1)} %param.37) | copy-start | bytes 786436
  32.6 70.7 %copy-start.14 = (bf16[256,512]{1,0:T(8,128)(2,1)S(1)}, bf16[256,512]{1,0:T(8,128)(2,1)}, u32[]{:S(2)}) copy-start(bf16[256,512]{1,0:T(8,128)(2,1)} %param.40) | copy-start | bytes 786436
  32.6 54.1 %all-to-all-start = ((bf16[16,12,1024]{2,1,0:T(8,128)(2,1)}), bf16[16,12,1024]{2,1,0:T(8,128)(2,1)S(1)}, u32[]{:S(2)}, u32[]{:S(2)}) async-start(bf16[16,12,1024]{2,1,0:T(8,128)(2,1)} %copy.73), calls=%async_computation.1 | async-start | bytes 1048576 | tf_op jit(solution)/shard_map/all_to_all | solution.py:162
  40.8 61.5 %all-reduce.2.cloned.1.call-start = ((), (), s32[]{:S(2)}) async-start(), calls=%async_computation.4 | async-start | bytes 524288 | tf_op jit(solution)/shard_map/psum | solution.py:46
  85.9 36.2 %copy-start.10 = (bf16[16,6]{0,1:T(8,128)(2,1)S(1)}, bf16[16,6]{0,1:T(8,128)(2,1)}, u32[]{:S(2)}) copy-start(bf16[16,6]{0,1:T(8,128)(2,1)} %param.34) | copy-start | bytes 580
  86.6 35.6 %copy-start.15 = (f32[1024]{0:T(1024)S(1)}, f32[1024]{0:T(1024)}, u32[]{:S(2)}) copy-start(f32[1024]{0:T(1024)} %param.41) | copy-start | bytes 12292
  86.7 27.0 %reduce-scatter.5.cloned.1.call-start = ((), (), s32[]{:S(2)}) async-start(), calls=%async_computation.6 | async-start | bytes 589824 | tf_op jit(solution)/shard_map/reduce_scatter | solution.py:40
  88.4 106.4 %reduce-scatter.3.cloned.1.call-start = ((), (), s32[]{:S(2)}) async-start(), calls=%async_computation.5 | async-start | bytes 557056 | tf_op jit(solution)/shard_map/reduce_scatter | solution.py:184
  115.4 79.4 %all-to-all-start.1 = ((bf16[16,12,512]{2,1,0:T(8,128)(2,1)}), bf16[16,12,512]{2,1,0:T(8,128)(2,1)S(1)}, u32[]{:S(2)}, u32[]{:S(2)}) async-start(bf16[16,12,512]{2,1,0:T(8,128)(2,1)} %copy.75), calls=%async_computation.3 | async-start | bytes 524288 | tf_op jit(solution)/shard_map/all_to_all | solution.py:167
Sparse Core Ops, SparseCore 0:
  86.8 15.5 all-reduce.1
  104.6 9.0 reduce-scatter.4
  115.9 78.8 reduce-scatter.2
where the time goes:
time: 204 us; the launch traced here: 203 us
  waiting for transfers between devices  95.6 us (47%)
  blocking collectives  48.2 us (24%)
  starting transfers between devices  15 us (7%)
  matrix products  14.8 us (7%)
  between operations  13.5 us (7%)
  local copies, waits for them, and re-layouts  10.3 us (5%)
  other arithmetic  5.81 us (3%)
    reduce_scatter x1, waiting for transfers between devices, shards(): lax.psum_scatter(branch_term, 'ep', scatter_dimension=0, tiled=True)  72.4 us
    all_gather x1, blocking collectives, shards(): piece_rows = lax.all_gather(input_half, 'ep', axis=0, tiled=True)  44.5 us
    psum x1, waiting for transfers between devices, dense_branch(): summed = lax.psum(partials.astype(jnp.bfloat16), 'tp').astype(jnp.float32)  13.9 us
    reduce_scatter x1, waiting for transfers between devices, expert_rows(): lax.psum_scatter(partial_value.astype(jnp.bfloat16), 'tp', scatter_dimens...  9.22 us
    all_to_all x1, starting transfers between devices, shards(): lax.all_to_all(outgoing, 'ep', split_axis=0, concat_axis=0, tiled=True)  8.15 us
    all_to_all x1, starting transfers between devices, shards(): lax.all_to_all(expert_out, 'ep', split_axis=0, concat_axis=0, tiled=True)  6.71 us
    unnamed x33, local copies, waits for them, and re-layouts  6.48 us
  transfers between devices with their start and end apart: 5, of which 3 were waited for; matrix products, arithmetic and copies ran while one was open for 3% of the time, Pallas kernels for 0%

commit v1 on v0

--- a/solution.py
+++ b/solution.py
@@ -43,7 +43,9 @@
 
 
 def dense_branch(partials, dense_down):
-    summed = lax.psum(partials.astype(jnp.bfloat16), "tp").astype(jnp.float32)
+    summed = jnp.sum(lax.all_gather(partials.astype(jnp.bfloat16), "tp"), axis=0).astype(
+        jnp.float32
+    )
     unit_count = partials.shape[1] // 2
     dense_hidden = (jax.nn.silu(summed[:, :unit_count]) * summed[:, unit_count:]).astype(
         jnp.bfloat16

time: 204 us -> 185 us (0.907)
  waiting for transfers between devices: 95.6 us -> 83.6 us
  starting transfers between devices: 15 us -> 11.6 us
  blocking collectives: 48.2 us -> 45.4 us
    all_to_all x1, waiting for transfers between devices: 0.01 us -> 15.4 us  [shards(): lax.all_to_all(outgoing, 'ep', split_axis=0, concat_axis=0, tiled=True)]
    psum x1 -> x0, waiting for transfers between devices: 13.9 us -> none  [dense_branch(): summed = lax.psum(partials.astype(jnp.bfloat16), 'tp').astype(jnp.float32)]
    reduce_scatter x1, waiting for transfers between devices: 9.22 us -> 0.02 us  [expert_rows(): lax.psum_scatter(partial_value.astype(jnp.bfloat16), 'tp', scatter_dimens...]
    all_gather x1, blocking collectives: 44.5 us -> 39.5 us  [shards(): piece_rows = lax.all_gather(input_half, 'ep', axis=0, tiled=True)]
    reduce_scatter x1, waiting for transfers between devices: 72.4 us -> 68.2 us  [shards(): lax.psum_scatter(branch_term, 'ep', scatter_dimension=0, tiled=True)]
    all_to_all x1, starting transfers between devices: 6.71 us -> 3.53 us  [shards(): lax.all_to_all(expert_out, 'ep', split_axis=0, concat_axis=0, tiled=True)]
    all_gather x0 -> x1, blocking collectives: none -> 2.18 us  [dense_branch(): lax.all_gather(partials.astype(jnp.bfloat16), 'tp')]
    unnamed x33 -> x34, local copies, waits for them, and re-layouts: 6.48 us -> 6.62 us
  transfers between devices with their start and end apart: 5 -> 4, of which waited for: 3 -> 2; matrix products, arithmetic and copies ran while one was open for 3% -> 2% of each run, Pallas kernels for 0% -> 0%
where the time goes in v1:
time: 185 us; the launch traced here: 184 us
  waiting for transfers between devices  83.6 us (45%)
  blocking collectives  45.4 us (25%)
  matrix products  14.8 us (8%)
  between operations  13.8 us (7%)
  starting transfers between devices  11.6 us (6%)
  local copies, waits for them, and re-layouts  10.6 us (6%)
  other arithmetic  4.25 us (2%)
    reduce_scatter x1, waiting for transfers between devices, shards(): lax.psum_scatter(branch_term, 'ep', scatter_dimension=0, tiled=True)  68.2 us
    all_gather x1, blocking collectives, shards(): piece_rows = lax.all_gather(input_half, 'ep', axis=0, tiled=True)  39.5 us
    all_to_all x1, waiting for transfers between devices, shards(): lax.all_to_all(outgoing, 'ep', split_axis=0, concat_axis=0, tiled=True)  15.4 us
    all_to_all x1, starting transfers between devices, shards(): lax.all_to_all(outgoing, 'ep', split_axis=0, concat_axis=0, tiled=True)  8.02 us
    unnamed x34, local copies, waits for them, and re-layouts  6.62 us
    psum x1, blocking collectives, shards(): lax.psum(attn_part.astype(jnp.bfloat16), 'tp').astype(jnp.float32)  3.72 us
  transfers between devices with their start and end apart: 4, of which 2 were waited for; matrix products, arithmetic and copies ran while one was open for 2% of the time, Pallas kernels for 0%

profile of v1, /device:TPU:0, one launch (start us, length us, event | category | flops | bytes accessed | tf_op | source)
XLA Modules:
  0.0 184.1 jit_solution(3862367035761697274)
XLA Ops:
  6.5 0.7 convert_element_type.109
  7.3 0.7 iota_compare_fusion
  8.0 0.9 fusion.34
  8.9 1.2 fusion.61
  10.2 1.6 fusion.63
  12.3 0.2 fusion.47
  12.6 6.4 %copy.67 = bf16[16,1024,128]{1,2,0:T(8,128)(2,1)} copy(bf16[16,1024,128]{2,1,0:T(8,128)(2,1)} %param.29) | data formatting | bytes 8388608 | tf_op args[8]
  19.1 3.0 %fusion.67 = (f32[16,4,2]{1,2,0:T(2,128)S(1)}, f32[16,1,4,2,1024]{4,2,3,0,1:T(4,128)S(1)}) fusion(bf16[16,1024,2,64]{1,3,2,0:T(8,128)(2,1)} %bitcast.155, bf16[16,4,2,32]{3,1,2,0:T(4,128)(2,1)S(1)} %copy.66, bf16[16,4,2,32]{3,1,2,0:T(4,128)(2,1)S(1)} %copy.65, pred[16,1024]{1,0:T(8,128)(4,1)S(1)} %iota_compare_fusion), kind=kOutput, calls=%fused_computation.108 | convolution fusion | flops 17203072 | bytes 4751872 | tf_op jit(solution)/shard_map/sgjcd,slgcd->sgjcl/dot_general | solution.py:108
  22.3 0.3 fusion.15
  22.9 0.3 fusion.14
  23.4 0.2 fusion.9
  23.6 3.0 %multiply_reduce_fusion = (f32[16,4]{1,0:T(8,128)S(1)}, f32[16,4,128]{2,1,0:T(4,128)S(1)}) fusion(f32[16,128]{1,0:T(8,128)S(1)} %fusion.9, f32[16,4]{1,0:T(8,128)S(1)} %copy.73, bf16[16,1024,128]{2,1,0:T(8,128)(2,1)} %param.30, f32[16,1,4,2,1024]{4,2,3,0,1:T(4,128)S(1)} %fusion.14, f32[4]{0:T(128)S(1)} %copy-done.9), kind=kOutput, calls=%fused_computation.71 | convolution fusion | flops 17006528 | bytes 4760080 | tf_op jit(solution)/shard_map/sgjl,slgv->sgjv/dot_general | solution.py:127
  26.7 0.2 convolution_convert_fusion.3
  27.0 3.7 %psum.7 = bf16[16,1024]{1,0:T(8,128)(2,1)S(1)} all-reduce(bf16[16,1024]{1,0:T(8,128)(2,1)S(1)} %convolution_convert_fusion.3), channel_id=1, replica_groups=mesh['ep'=16,'tp'=2] {'tp'}, use_global_device_ids=true, to_apply=%region_4.5 | all-reduce | flops 16384 | bytes 65536 | tf_op jit(solution)/shard_map/psum | solution.py:139
  31.3 0.2 fusion.68
  31.6 1.0 copy.77
  32.6 8.0 %all-to-all-start = ((bf16[16,12,1024]{2,1,0:T(8,128)(2,1)}), bf16[16,12,1024]{2,1,0:T(8,128)(2,1)S(1)}, u32[]{:S(2)}, u32[]{:S(2)}) async-start(bf16[16,12,1024]{2,1,0:T(8,128)(2,1)} %copy.77), calls=%async_computation.1 | async-start | bytes 1048576 | tf_op jit(solution)/shard_map/all_to_all | solution.py:164
  40.7 15.4 %all-to-all-done = bf16[16,12,1024]{2,1,0:T(8,128)(2,1)S(1)} async-done(((bf16[16,12,1024]{2,1,0:T(8,128)(2,1)}), bf16[16,12,1024]{2,1,0:T(8,128)(2,1)S(1)}, u32[]{:S(2)}, u32[]{:S(2)}) %all-to-all-start) | async-done | bytes 393248 | tf_op jit(solution)/shard_map/all_to_all | solution.py:164
  56.2 0.2 fusion.22
  56.5 0.3 fusion.5
  56.8 1.0 convolution_convert_fusion
  57.9 39.5 %all_gather.7 = bf16[256,512]{1,0:T(8,128)(2,1)S(1)} all-gather(bf16[16,512]{1,0:T(8,128)(2,1)S(1)} %constant_dynamic-slice_fusion), channel_id=1, replica_groups=mesh['ep'=16,'tp'=2] {'ep'}, dimensions={0}, use_global_device_ids=true | all-gather | bytes 278528 | tf_op jit(solution)/shard_map/all_gather | solution.py:177
  97.4 0.3 fusion.3
  97.7 0.3 fusion.4
  98.0 0.1 copy.74
  98.1 2.2 %all_gather.8 = bf16[2,256,512]{2,1,0:T(8,128)(2,1)S(1)} all-gather(bf16[1,256,512]{2,1,0:T(8,128)(2,1)S(1)} %copy.74), channel_id=1, replica_groups=mesh['ep'=16,'tp'=2] {'tp'}, dimensions={0}, use_global_device_ids=true | all-gather | bytes 786432 | tf_op jit(solution)/shard_map/all_gather | solution.py:46
  100.4 0.1 copy.83
  100.6 1.1 fusion.26
  101.7 1.7 copy.79
  103.5 3.5 %all-to-all-start.1 = ((bf16[16,12,512]{2,1,0:T(8,128)(2,1)}), bf16[16,12,512]{2,1,0:T(8,128)(2,1)S(1)}, u32[]{:S(2)}, u32[]{:S(2)}) async-start(bf16[16,12,512]{2,1,0:T(8,128)(2,1)} %copy.79), calls=%async_computation.3 | async-start | bytes 524288 | tf_op jit(solution)/shard_map/all_to_all | solution.py:169
  107.3 68.2 %reduce-scatter.3.cloned.1.call-done = f32[16,512]{1,0:T(8,128)} async-done(((f32[256,512]{1,0:T(8,128)}), f32[16,512]{1,0:T(8,128)}) %reduce-scatter.3.cloned.1.call-update) | async-done | bytes 32784 | tf_op jit(solution)/shard_map/reduce_scatter | solution.py:186
  175.4 1.8 fusion.8
  (80 shorter events, 2.6 us)
Async XLA Ops:
  6.5 20.2 %copy-start = (bf16[512,1024]{1,0:T(8,128)(2,1)S(1)}, bf16[512,1024]{1,0:T(8,128)(2,1)}, u32[]{:S(2)}) copy-start(bf16[512,1024]{1,0:T(8,128)(2,1)} %param.28) | copy-start | bytes 3145732
  19.1 4.1 %copy-start.9 = (f32[4]{0:T(128)S(1)}, f32[4]{0:T(128)}, u32[]{:S(2)}) copy-start(f32[4]{0:T(128)} %param.26) | copy-start | bytes 52
  19.1 4.3 %copy-start.1 = (bf16[16,1024]{1,0:T(8,128)(2,1)S(1)}, bf16[16,1024]{1,0:T(8,128)(2,1)}, u32[]{:S(2)}) copy-start(bf16[16,1024]{1,0:T(8,128)(2,1)} %param.21) | copy-start | bytes 98308
  19.1 4.3 %copy-start.7 = (f32[1024]{0:T(1024)S(1)}, f32[1024]{0:T(1024)}, u32[]{:S(2)}) copy-start(f32[1024]{0:T(1024)} %param.22) | copy-start | bytes 12292
  19.1 4.3 %copy-start.12 = (bf16[1024,128]{1,0:T(8,128)(2,1)S(1)}, bf16[1024,128]{1,0:T(8,128)(2,1)}, u32[]{:S(2)}) copy-start(bf16[1024,128]{1,0:T(8,128)(2,1)} %param.25) | copy-start | bytes 786436
  22.1 4.5 %copy-start.11 = (f32[128]{0:T(128)S(1)}, f32[128]{0:T(128)}, u32[]{:S(2)}) copy-start(f32[128]{0:T(128)} %param.27) | copy-start | bytes 1540
  22.1 8.7 %copy-start.6 = (s32[16,6]{0,1:T(8,128)S(1)}, s32[16,6]{0,1:T(8,128)}, u32[]{:S(2)}) copy-start(s32[16,6]{0,1:T(8,128)} %param.33) | copy-start | bytes 1156
  22.1 9.0 %copy-start.8 = (f32[1024]{0:T(1024)S(1)}, f32[1024]{0:T(1024)}, u32[]{:S(2)}) copy-start(f32[1024]{0:T(1024)} %param.32) | copy-start | bytes 12292
  26.6 29.7 %copy-start.2 = (bf16[1,1024,128]{2,1,0:T(8,128)(2,1)S(1)}, bf16[1,1024,128]{2,1,0:T(8,128)(2,1)}, u32[]{:S(2)}) copy-start(bf16[1,1024,128]{2,1,0:T(8,128)(2,1)} %param.35) | copy-start | bytes 786436
  26.6 29.9 %copy-start.13 = (bf16[1,1024,128]{2,1,0:T(8,128)(2,1)S(1)}, bf16[1,1024,128]{2,1,0:T(8,128)(2,1)}, u32[]{:S(2)}) copy-start(bf16[1,1024,128]{2,1,0:T(8,128)(2,1)} %param.36) | copy-start | bytes 786436
  26.6 30.2 %copy-start.5 = (bf16[1,128,1024]{2,1,0:T(8,128)(2,1)S(1)}, bf16[1,128,1024]{2,1,0:T(8,128)(2,1)}, u32[]{:S(2)}) copy-start(bf16[1,128,1024]{2,1,0:T(8,128)(2,1)} %param.37) | copy-start | bytes 786436
  31.0 66.4 %copy-start.3 = (bf16[512,256]{1,0:T(8,128)(2,1)S(1)}, bf16[512,256]{1,0:T(8,128)(2,1)}, u32[]{:S(2)}) copy-start(bf16[512,256]{1,0:T(8,128)(2,1)} %param.38) | copy-start | bytes 786436
  31.5 66.2 %copy-start.4 = (bf16[512,256]{1,0:T(8,128)(2,1)S(1)}, bf16[512,256]{1,0:T(8,128)(2,1)}, u32[]{:S(2)}) copy-start(bf16[512,256]{1,0:T(8,128)(2,1)} %param.39) | copy-start | bytes 786436
  32.6 23.5 %all-to-all-start = ((bf16[16,12,1024]{2,1,0:T(8,128)(2,1)}), bf16[16,12,1024]{2,1,0:T(8,128)(2,1)S(1)}, u32[]{:S(2)}, u32[]{:S(2)}) async-start(bf16[16,12,1024]{2,1,0:T(8,128)(2,1)} %copy.77), calls=%async_computation.1 | async-start | bytes 1048576 | tf_op jit(solution)/shard_map/all_to_all | solution.py:164
  40.6 61.1 %reduce-scatter.5.cloned.1.call-start = ((), (), s32[]{:S(2)}) async-start(), calls=%async_computation.5 | async-start | bytes 589824 | tf_op jit(solution)/shard_map/reduce_scatter | solution.py:40
  56.2 44.4 %copy-start.14 = (bf16[256,512]{1,0:T(8,128)(2,1)S(1)}, bf16[256,512]{1,0:T(8,128)(2,1)}, u32[]{:S(2)}) copy-start(bf16[256,512]{1,0:T(8,128)(2,1)} %param.40) | copy-start | bytes 786436
  57.8 117.6 %reduce-scatter.3.cloned.1.call-start = ((), (), s32[]{:S(2)}) async-start(), calls=%async_computation.4 | async-start | bytes 557056 | tf_op jit(solution)/shard_map/reduce_scatter | solution.py:186
  97.4 9.6 %copy-start.10 = (bf16[16,6]{0,1:T(8,128)(2,1)S(1)}, bf16[16,6]{0,1:T(8,128)(2,1)}, u32[]{:S(2)}) copy-start(bf16[16,6]{0,1:T(8,128)(2,1)} %param.34) | copy-start | bytes 580
  97.4 9.8 %copy-start.15 = (f32[1024]{0:T(1024)S(1)}, f32[1024]{0:T(1024)}, u32[]{:S(2)}) copy-start(f32[1024]{0:T(1024)} %param.41) | copy-start | bytes 12292
  103.5 71.9 %all-to-all-start.1 = ((bf16[16,12,512]{2,1,0:T(8,128)(2,1)}), bf16[16,12,512]{2,1,0:T(8,128)(2,1)S(1)}, u32[]{:S(2)}, u32[]{:S(2)}) async-start(bf16[16,12,512]{2,1,0:T(8,128)(2,1)} %copy.79), calls=%async_computation.3 | async-start | bytes 524288 | tf_op jit(solution)/shard_map/all_to_all | solution.py:169
Sparse Core Ops, SparseCore 0:
  57.9 6.2 reduce-scatter.4
  101.8 73.5 reduce-scatter.2
